TPU v7x, 512 devices: a whole 4x4x16 slice. The times are simulated.
512 devices in a mesh: ep: 16 (over y, x), tp: 32 (over z, core).
Axes of the slice: x: 4, y: 4, z: 16, core: 2. Of those that a mesh axis runs over, the one named last changes fastest.
Arguments:
- tokens: bfloat16 [4096, 2048], P('ep', 'tp'), may hold values from -600 to 600
- pre_gain: float32 [2048], P('tp'), may hold values from 0.1 to 1.9
- expert_gate: bfloat16 [16, 2048, 8192], P('ep', None, 'tp'), may hold values from -0.125 to 0.125
- expert_up: bfloat16 [16, 2048, 8192], P('ep', None, 'tp'), may hold values from -0.125 to 0.125
- expert_down: bfloat16 [16, 8192, 2048], P('ep', 'tp'), may hold values from -8 to 8
- routes: int32 [4096, 2], P('ep'), may hold values from 0 to 15, all different within a row; in each aligned block of 256 rows (0 to 255, 256 to 511, ...) at most 48 rows name the same one
- route_weights: float32 [4096, 2], P('ep'), may hold values from 0.1 to 1
- post_gain: float32 [2048], P('tp'), may hold values from 0.1 to 1.9
Outputs:
- layer_out: bfloat16 [4096, 2048], P('ep', 'tp')
Inputs may be any that keep to these rules, and one draw needn't show every extreme that they name: `routes`: each token names 2 different experts. Among the 256 tokens of one index of ep no expert is named more than 48 times, a bound that some expert reaches in some of these blocks.
All inputs are finite; a program needn't handle non-finite values.
Results may differ from a plain program's by a relative error of at most 0.024.
Values may be sent and summed in bfloat16 or wider, within the bound.
No kernel may reach another device: no remote copies, remote signals or barrier semaphores. Data moves between devices by JAX's collectives and lax.ppermute only.
A program may use at most 64 MiB of HBM per device.

v0:
```python
import jax
import jax.numpy as jnp
from jax import lax
from jax.sharding import Mesh
from jax.sharding import PartitionSpec as P

TP = ("tp_0", "tp_1")
EPSILON = 1e-06


def sent_to_all(value, axis):
    copies = jnp.broadcast_to(value, (lax.axis_size(axis), *value.shape))
    return lax.all_to_all(copies, axis, split_axis=0, concat_axis=0, tiled=True)


def taken_together(value, axis):
    everything = sent_to_all(value, axis)
    return jnp.sum(everything, axis=0)


def own_block(parts, axes, turns):
    lengths = [lax.axis_size(a) for a in axes]
    parts = parts.reshape(*lengths, *parts.shape[1:])
    parts = parts.transpose(*turns, *range(len(axes), parts.ndim))
    parts = parts.reshape(-1, *parts.shape[len(axes) :])
    for k in turns:
        parts = lax.psum_scatter(parts, axes[k], scatter_dimension=0, tiled=True)
    return parts[0]


def split_up(value, dim, peers):
    before, after = (value.shape[:dim], value.shape[dim + 1 :])
    return jnp.moveaxis(value.reshape(*before, peers, -1, *after), dim, 0)


def summed_rows(value, axes, turns, dim):
    peers = lax.axis_size(axes)
    return own_block(split_up(value, dim, peers), axes, turns)


def local(tokens, pre_gain, expert_gate, expert_up, expert_down, routes, route_weights, post_gain):
    local_experts = expert_gate.shape[0]
    groups = lax.axis_size("ep")
    experts_all = local_experts * groups
    tok_rows, part_width = tokens.shape
    full_width = part_width * lax.axis_size(TP)
    capacity = 3 * tok_rows // experts_all
    values = tokens.astype(jnp.float32)
    input_sq = taken_together(jnp.sum(values * values, axis=-1), TP)
    normed = (
        values * lax.rsqrt(input_sq / full_width + EPSILON)[:, None] * pre_gain[None, :]
    ).astype(jnp.bfloat16)
    onehot = (routes[:, :, None] == jnp.arange(experts_all, dtype=jnp.int32)).astype(jnp.int32)
    onehot = onehot.reshape(tok_rows * 2, experts_all)
    earlier = jnp.cumsum(onehot, axis=0) - onehot
    slots = jnp.sum(earlier * onehot, axis=-1).reshape(tok_rows, 2)
    positions = routes * capacity + slots
    places = jnp.arange(experts_all * capacity, dtype=jnp.int32)
    first_pick = (places[:, None] == positions[None, :, 0]).astype(jnp.bfloat16)
    second_pick = (places[:, None] == positions[None, :, 1]).astype(jnp.bfloat16)
    dispatch = first_pick + second_pick
    outgoing = jnp.dot(dispatch, normed, preferred_element_type=jnp.float32).astype(jnp.bfloat16)
    arrived = lax.all_to_all(outgoing, "ep", split_axis=0, concat_axis=0, tiled=True)
    fragment = lax.all_gather(arrived, TP, axis=1, tiled=True)
    count = fragment.shape[1]
    grouped = fragment.reshape(groups, local_experts, capacity, count)
    gate_pre = jnp.einsum(
        "secw,ewf->secf", grouped, expert_gate, preferred_element_type=jnp.float32
    )
    up_pre = jnp.einsum("secw,ewf->secf", grouped, expert_up, preferred_element_type=jnp.float32)
    hidden = (jax.nn.silu(gate_pre) * up_pre).astype(jnp.bfloat16)
    product = jnp.einsum("secf,efd->dsec", hidden, expert_down, preferred_element_type=jnp.float32)
    summed = summed_rows(
        product.reshape(part_width * lax.axis_size(TP), groups * local_experts * capacity).astype(
            jnp.bfloat16
        ),
        TP,
        (1, 0),
        0,
    ).astype(jnp.float32)
    expert_out = summed.astype(jnp.bfloat16)
    returned = lax.all_to_all(expert_out, "ep", split_axis=1, concat_axis=1, tiled=True)
    contract = (((0,), (1,)), ((), ()))
    first_out = lax.dot_general(first_pick, returned, contract, preferred_element_type=jnp.float32)
    second_out = lax.dot_general(
        second_pick, returned, contract, preferred_element_type=jnp.float32
    )
    combined = route_weights[:, 0:1] * first_out + route_weights[:, 1:2] * second_out
    output_sq = taken_together(jnp.sum(combined * combined, axis=-1), TP)
    scaled = combined * lax.rsqrt(output_sq / full_width + EPSILON)[:, None] * post_gain[None, :]
    return scaled.astype(jnp.bfloat16)


def solution(mesh):
    torus = Mesh(mesh.devices.reshape(mesh.shape["ep"], 16, 2), ("ep", "tp_0", "tp_1"))
    in_specs = (
        P("ep", TP),
        P(TP),
        P("ep", None, TP),
        P("ep", None, TP),
        P("ep", TP, None),
        P("ep", None),
        P("ep", None),
        P(TP),
    )
    out_specs = P("ep", TP)
    return jax.shard_map(local, mesh=torus, in_specs=in_specs, out_specs=out_specs, check_vma=False)
```

profile of v0, /device:TPU:1, one launch (start us, length us, event | category | flops | bytes accessed | tf_op | source)
XLA Modules:
  0.0 277.1 jit_solution(4352224880434988949)
XLA Ops:
  6.5 0.9 fusion.16
  7.4 0.6 broadcast_in_dim.4
  8.0 16.7 %all-to-all-start = ((f32[32,1,256]{2,1,0:T(1,128)}), f32[32,1,256]{2,1,0:T(1,128)S(1)}, u32[]{:S(2)}, u32[]{:S(2)}) async-start(f32[32,1,256]{2,1,0:T(1,128)} %broadcast_in_dim.4), calls=%async_computation | async-start | bytes 65536 | tf_op jit(solution)/shard_map/all_to_all | solution.py:13
  24.8 0.8 copy.64
  26.0 1.2 reduce-window.6
  27.1 0.2 slice_reduce_fusion
  27.7 0.7 multiply_add_fusion
  28.4 8.4 %all-to-all-done = f32[32,1,256]{2,1,0:T(1,128)S(1)} async-done(((f32[32,1,256]{2,1,0:T(1,128)}), f32[32,1,256]{2,1,0:T(1,128)S(1)}, u32[]{:S(2)}, u32[]{:S(2)}) %all-to-all-start) | async-done | bytes 32800 | tf_op jit(solution)/shard_map/all_to_all | solution.py:13
  36.9 1.1 convolution_convert_fusion.1
  38.0 0.2 copy.77
  38.2 0.2 reshape.84
  38.3 13.2 %all_to_all.36 = bf16[16,2,1536]{2,1,0:T(2,128)(2,1)S(1)} all-to-all(bf16[16,2,1536]{2,1,0:T(2,128)(2,1)S(1)} %reshape.84), channel_id=1, replica_groups=mesh['ep'=16,'tp_0'=16,'tp_1'=2] {'ep'}, dimensions={0} | all-to-all | bytes 196608 | tf_op jit(solution)/shard_map/all_to_all | solution.py:63
  51.5 0.2 reshape.85
  51.7 0.8 copy.78
  52.6 63.2 %all-gather.2.cloned.1.call-done = bf16[768,2048]{0,1:T(8,128)(2,1)} async-done(((bf16[768,64]{0,1:T(8,128)(2,1)}), bf16[768,2048]{0,1:T(8,128)(2,1)}) %all-gather.2.cloned.1.call-update) | async-done | bytes 3145744 | tf_op jit(solution)/shard_map/all_gather | solution.py:64
  115.7 4.7 %copy.71 = bf16[768,2048]{1,0:T(8,128)(2,1)} copy(bf16[768,2048]{0,1:T(8,128)(2,1)} %all-gather.2.cloned.1.call-done) | data formatting | bytes 6291456 | tf_op jit(solution)/shard_map/all_gather | solution.py:64
  120.4 3.0 %convolution_bitcast_fusion.1 = f32[16,1,48,256]{3,2,0,1:T(8,128)S(1)} fusion(bf16[16,48,2048]{2,1,0:T(8,128)(2,1)} %bitcast.71, bf16[1,2048,256]{2,1,0:T(8,128)(2,1)S(1)} %copy-done.4), kind=kOutput, calls=%fused_computation.3 | convolution fusion | flops 805306368 | bytes 4980736 | tf_op jit(solution)/shard_map/secw,ewf->secf/dot_general | solution.py:67
  123.6 1.0 fusion.2
  124.6 2.7 fusion
  127.3 4.6 %copy.72 = bf16[2048,768]{1,0:T(8,128)(2,1)} copy(bf16[2048,768]{0,1:T(8,128)(2,1)} %fusion) | data formatting | bytes 6291456 | tf_op jit(solution)/shard_map/convert_element_type | solution.py:74
  131.9 3.9 %copy.73 = bf16[2,16,64,768]{3,2,1,0:T(8,128)(2,1)} copy(bf16[2,16,64,768]{3,2,0,1:T(8,128)(2,1)} %bitcast.70) | data formatting | bytes 6291456 | tf_op jit(solution)/shard_map/transpose | solution.py:24
  135.9 18.9 %reduce-scatter.3.cloned.1.call-done = bf16[16,64,768]{2,1,0:T(8,128)(2,1)} async-done(((bf16[32,64,768]{2,1,0:T(8,128)(2,1)}), bf16[16,64,768]{2,1,0:T(8,128)(2,1)}) %reduce-scatter.3.cloned.1.call-update) | async-done | bytes 1572880 | tf_op jit(solution)/shard_map/reduce_scatter | solution.py:27
  154.8 66.2 %reduce-scatter.5.cloned.1.call-done = bf16[1,64,768]{2,1,0:T(8,128)(2,1)} async-done(((bf16[16,64,768]{2,1,0:T(8,128)(2,1)}), bf16[1,64,768]{2,1,0:T(8,128)(2,1)}) %reduce-scatter.5.cloned.1.call-update) | async-done | bytes 98320 | tf_op jit(solution)/shard_map/reduce_scatter | solution.py:27
  221.0 1.1 copy.79
  222.1 0.8 reshape.86
  222.9 6.4 %all-to-all-start.2 = ((bf16[16,2,1536]{2,1,0:T(2,128)(2,1)}), bf16[16,2,1536]{2,1,0:T(2,128)(2,1)S(1)}, u32[]{:S(2)}, u32[]{:S(2)}) async-start(bf16[16,2,1536]{2,1,0:T(2,128)(2,1)} %reshape.86), calls=%async_computation.4 | async-start | bytes 196608 | tf_op jit(solution)/shard_map/all_to_all | solution.py:82
  229.4 6.6 %all-to-all-done.2 = bf16[16,2,1536]{2,1,0:T(2,128)(2,1)S(1)} async-done(((bf16[16,2,1536]{2,1,0:T(2,128)(2,1)}), bf16[16,2,1536]{2,1,0:T(2,128)(2,1)S(1)}, u32[]{:S(2)}, u32[]{:S(2)}) %all-to-all-start.2) | async-done | bytes 98336 | tf_op jit(solution)/shard_map/all_to_all | solution.py:82
  236.0 0.2 reshape.87
  236.2 0.3 convolution_multiply_fusion.1
  236.5 0.3 multiply_reduce_fusion
  236.8 33.0 %all_to_all.37 = f32[32,1,256]{2,1,0:T(1,128)S(1)} all-to-all(f32[32,1,256]{2,1,0:T(1,128)S(1)} %broadcast_in_dim.5), channel_id=1, replica_groups=mesh['ep'=16,'tp_0'=16,'tp_1'=2] {'tp_0','tp_1'}, dimensions={0} | all-to-all | bytes 65536 | tf_op jit(solution)/shard_map/all_to_all | solution.py:13
  269.9 0.7 multiply_convert_fusion
  (33 shorter events, 1.1 us)
Async XLA Ops:
  6.5 118.0 %copy-start = (bf16[1,256,2048]{2,1,0:T(8,128)(2,1)S(1)}, bf16[1,256,2048]{2,1,0:T(8,128)(2,1)}, u32[]{:S(2)}) copy-start(bf16[1,256,2048]{2,1,0:T(8,128)(2,1)} %param.12) | copy-start | bytes 3145732
  8.0 28.8 %all-to-all-start = ((f32[32,1,256]{2,1,0:T(1,128)}), f32[32,1,256]{2,1,0:T(1,128)S(1)}, u32[]{:S(2)}, u32[]{:S(2)}) async-start(f32[32,1,256]{2,1,0:T(1,128)} %broadcast_in_dim.4), calls=%async_computation | async-start | bytes 65536 | tf_op jit(solution)/shard_map/all_to_all | solution.py:13
  24.8 90.9 %all-gather.2.cloned.1.call-start = ((), (), s32[]{:S(2)}) async-start(), calls=%async_computation.6 | async-start | bytes 3244032 | tf_op jit(solution)/shard_map/all_gather | solution.py:64
  52.5 67.9 %copy-start.4 = (bf16[1,2048,256]{2,1,0:T(8,128)(2,1)S(1)}, bf16[1,2048,256]{2,1,0:T(8,128)(2,1)}, u32[]{:S(2)}) copy-start(bf16[1,2048,256]{2,1,0:T(8,128)(2,1)} %param.10) | copy-start | bytes 3145732
  52.5 102.3 %reduce-scatter.3.cloned.1.call-start = ((), (), s32[]{:S(2)}) async-start(), calls=%async_computation.7 | async-start | bytes 4718592 | tf_op jit(solution)/shard_map/reduce_scatter | solution.py:27
  120.4 3.1 %copy-start.1 = (bf16[768,2048]{1,0:T(8,128)(2,1)S(1)}, bf16[768,2048]{1,0:T(8,128)(2,1)}, u32[]{:S(2)}) copy-start(bf16[768,2048]{1,0:T(8,128)(2,1)} %copy.71) | copy-start | bytes 9437188
  120.4 3.1 %copy-start.5 = (bf16[1,2048,256]{2,1,0:T(8,128)(2,1)S(1)}, bf16[1,2048,256]{2,1,0:T(8,128)(2,1)}, u32[]{:S(2)}) copy-start(bf16[1,2048,256]{2,1,0:T(8,128)(2,1)} %param.11) | copy-start | bytes 3145732
  135.8 93.5 %copy-start.2 = (f32[256,2]{0,1:T(2,128)S(1)}, f32[256,2]{0,1:T(2,128)}, u32[]{:S(2)}) copy-start(f32[256,2]{0,1:T(2,128)} %param.14) | copy-start | bytes 6148
  135.8 134.0 %copy-start.3 = (f32[64]{0:T(128)S(1)}, f32[64]{0:T(128)}, u32[]{:S(2)}) copy-start(f32[64]{0:T(128)} %param.15) | copy-start | bytes 772
  135.9 85.2 %reduce-scatter.5.cloned.1.call-start = ((), (), s32[]{:S(2)}) async-start(), calls=%async_computation.8 | async-start | bytes 1671168 | tf_op jit(solution)/shard_map/reduce_scatter | solution.py:27
  222.9 13.1 %all-to-all-start.2 = ((bf16[16,2,1536]{2,1,0:T(2,128)(2,1)}), bf16[16,2,1536]{2,1,0:T(2,128)(2,1)S(1)}, u32[]{:S(2)}, u32[]{:S(2)}) async-start(bf16[16,2,1536]{2,1,0:T(2,128)(2,1)} %reshape.86), calls=%async_computation.4 | async-start | bytes 196608 | tf_op jit(solution)/shard_map/all_to_all | solution.py:82
Sparse Core Ops, SparseCore 0:
  52.6 63.0 all-gather.1
  136.0 18.7 reduce-scatter.2
  157.6 63.3 reduce-scatter.4
where the time goes:
time: 278 us; the launch traced here: 277 us
  waiting for transfers between devices  163 us (59%)
  blocking collectives  46.2 us (17%)
  starting transfers between devices  23.3 us (8%)
  local copies, waits for them, and re-layouts  18.8 us (7%)
  between operations  13.3 us (5%)
  matrix products  8.38 us (3%)
  other arithmetic  3.68 us (1%)
    reduce_scatter x2, waiting for transfers between devices, own_block(): parts = lax.psum_scatter(parts, axes[k], scatter_dimension=0, tiled=True)  85.1 us
    all_gather x1, waiting for transfers between devices, local(): fragment = lax.all_gather(arrived, TP, axis=1, tiled=True)  63.2 us
    all_to_all x1, blocking collectives, sent_to_all(): return lax.all_to_all(copies, axis, split_axis=0, concat_axis=0, tiled=True)  33 us
    all_to_all x1, starting transfers between devices, sent_to_all(): return lax.all_to_all(copies, axis, split_axis=0, concat_axis=0, tiled=True)  16.7 us
    all_to_all x1, blocking collectives, local(): lax.all_to_all(outgoing, 'ep', split_axis=0, concat_axis=0, tiled=True)  13.2 us
    all_to_all x1, waiting for transfers between devices, sent_to_all(): return lax.all_to_all(copies, axis, split_axis=0, concat_axis=0, tiled=True)  8.44 us
    all_to_all x1, waiting for transfers between devices, local(): lax.all_to_all(expert_out, 'ep', split_axis=1, concat_axis=1, tiled=True)  6.64 us
    all_to_all x1, starting transfers between devices, local(): lax.all_to_all(expert_out, 'ep', split_axis=1, concat_axis=1, tiled=True)  6.45 us
  transfers between devices with their start and end apart: 5, of which 5 were waited for; matrix products, arithmetic and copies ran while one was open for 1% of the time, Pallas kernels for 0%

commit v1 on v0

--- a/solution.py
+++ b/solution.py
@@ -61,7 +61,8 @@
     dispatch = first_pick + second_pick
     outgoing = jnp.dot(dispatch, normed, preferred_element_type=jnp.float32).astype(jnp.bfloat16)
     arrived = lax.all_to_all(outgoing, "ep", split_axis=0, concat_axis=0, tiled=True)
-    fragment = lax.all_gather(arrived, TP, axis=1, tiled=True)
+    sent = jnp.stack([arrived] * lax.axis_size(TP))
+    fragment = jnp.concatenate(lax.all_to_all(sent, TP, 0, 0), axis=1)
     count = fragment.shape[1]
     grouped = fragment.reshape(groups, local_experts, capacity, count)
     gate_pre = jnp.einsum(

time: 278 us -> 373 us (1.34)
  blocking collectives: 46.2 us -> 198 us
  waiting for transfers between devices: 163 us -> 91.4 us
  local copies, waits for them, and re-layouts: 18.8 us -> 33.9 us
    all_to_all x0 -> x1, blocking collectives: none -> 152 us  [local(): fragment = jnp.concatenate(lax.all_to_all(sent, TP, 0, 0), axis=1)]
    all_gather x1 -> x0, waiting for transfers between devices: 63.2 us -> none  [local(): fragment = lax.all_gather(arrived, TP, axis=1, tiled=True)]
    another operation x1 -> x4, local copies, waits for them, and re-layouts: 0.01 us -> 10.3 us
    reshape x0 -> x1, local copies, waits for them, and re-layouts: none -> 10.2 us  [local(): fragment = jnp.concatenate(lax.all_to_all(sent, TP, 0, 0), axis=1)]
    reduce_scatter x2, waiting for transfers between devices: 85.1 us -> 76.2 us  [own_block(): parts = lax.psum_scatter(parts, axes[k], scatter_dimension=0, tiled=True)]
    all_gather x1 -> x0, local copies, waits for them, and re-layouts: 4.71 us -> none  [local(): fragment = lax.all_gather(arrived, TP, axis=1, tiled=True)]
  transfers between devices with their start and end apart: 5 -> 4, of which waited for: 5 -> 4; matrix products, arithmetic and copies ran while one was open for 1% -> 1% of each run, Pallas kernels for 0% -> 0%
where the time goes in v1:
time: 373 us; the launch traced here: 372 us
  blocking collectives  198 us (53%)
  waiting for transfers between devices  91.4 us (25%)
  local copies, waits for them, and re-layouts  33.9 us (9%)
  starting transfers between devices  23.4 us (6%)
  between operations  13.6 us (4%)
  matrix products  8.38 us (2%)
    all_to_all x1, blocking collectives, local(): fragment = jnp.concatenate(lax.all_to_all(sent, TP, 0, 0), axis=1)  152 us
    reduce_scatter x2, waiting for transfers between devices, own_block(): parts = lax.psum_scatter(parts, axes[k], scatter_dimension=0, tiled=True)  76.2 us
    all_to_all x1, blocking collectives, sent_to_all(): return lax.all_to_all(copies, axis, split_axis=0, concat_axis=0, tiled=True)  33 us
    all_to_all x1, starting transfers between devices, sent_to_all(): return lax.all_to_all(copies, axis, split_axis=0, concat_axis=0, tiled=True)  16.7 us
    all_to_all x1, blocking collectives, local(): lax.all_to_all(outgoing, 'ep', split_axis=0, concat_axis=0, tiled=True)  13.2 us
    reshape x1, local copies, waits for them, and re-layouts, local(): fragment = jnp.concatenate(lax.all_to_all(sent, TP, 0, 0), axis=1)  10.2 us
    another operation x2, local copies, waits for them, and re-layouts  9.83 us
    all_to_all x1, waiting for transfers between devices, sent_to_all(): return lax.all_to_all(copies, axis, split_axis=0, concat_axis=0, tiled=True)  8.44 us
  transfers between devices with their start and end apart: 4, of which 4 were waited for; matrix products, arithmetic and copies ran while one was open for 1% of the time, Pallas kernels for 0%

profile of v1, /device:TPU:1, one launch (start us, length us, event | category | flops | bytes accessed | tf_op | source)
XLA Modules:
  0.0 372.1 jit_solution(16903937679126898855)
XLA Ops:
  6.5 0.9 fusion.16
  7.4 0.6 broadcast_in_dim.4
  8.0 16.7 %all-to-all-start = ((f32[32,1,256]{2,1,0:T(1,128)}), f32[32,1,256]{2,1,0:T(1,128)S(1)}, u32[]{:S(2)}, u32[]{:S(2)}) async-start(f32[32,1,256]{2,1,0:T(1,128)} %broadcast_in_dim.4), calls=%async_computation | async-start | bytes 65536 | tf_op jit(solution)/shard_map/all_to_all | solution.py:13
  24.8 0.8 copy.64
  26.0 1.2 reduce-window.6
  27.1 0.2 slice_reduce_fusion
  27.7 0.7 multiply_add_fusion
  28.4 8.4 %all-to-all-done = f32[32,1,256]{2,1,0:T(1,128)S(1)} async-done(((f32[32,1,256]{2,1,0:T(1,128)}), f32[32,1,256]{2,1,0:T(1,128)S(1)}, u32[]{:S(2)}, u32[]{:S(2)}) %all-to-all-start) | async-done | bytes 32800 | tf_op jit(solution)/shard_map/all_to_all | solution.py:13
  36.9 1.1 convolution_convert_fusion.1
  38.0 0.2 copy.77
  38.2 0.2 reshape.90
  38.3 13.2 %all_to_all.38 = bf16[16,2,1536]{2,1,0:T(2,128)(2,1)S(1)} all-to-all(bf16[16,2,1536]{2,1,0:T(2,128)(2,1)S(1)} %reshape.90), channel_id=1, replica_groups=mesh['ep'=16,'tp_0'=16,'tp_1'=2] {'ep'}, dimensions={0} | all-to-all | bytes 196608 | tf_op jit(solution)/shard_map/all_to_all | solution.py:63
  51.9 0.3 stack.5
  52.2 151.6 %all_to_all.39 = bf16[32,768,64]{1,2,0:T(8,128)(2,1)} all-to-all(bf16[32,768,64]{1,2,0:T(8,128)(2,1)S(1)} %stack.5), channel_id=1, replica_groups=mesh['ep'=16,'tp_0'=16,'tp_1'=2] {'tp_0','tp_1'}, dimensions={0} | all-to-all | bytes 6291456 | tf_op jit(solution)/shard_map/all_to_all | solution.py:65
  203.8 10.2 %copy.71 = bf16[768,32,64]{2,1,0:T(8,128)(2,1)} copy(bf16[768,32,64]{0,2,1:T(8,128)(2,1)} %bitcast.71) | data formatting | bytes 6291456 | tf_op jit(solution)/shard_map/reshape | solution.py:65
  214.0 9.8 %reshape.82 = bf16[16,48,2048]{2,1,0:T(8,128)(2,1)} reshape(bf16[768,32,64]{2,1,0:T(8,128)(2,1)} %copy.71) | data formatting | bytes 6291456 | tf_op jit(solution)/shard_map/reshape.9
  223.8 3.0 convolution_bitcast_fusion.1
  227.0 1.0 fusion.2
  228.0 2.7 fusion
  230.7 4.6 %copy.72 = bf16[2048,768]{1,0:T(8,128)(2,1)} copy(bf16[2048,768]{0,1:T(8,128)(2,1)} %fusion) | data formatting | bytes 6291456 | tf_op jit(solution)/shard_map/convert_element_type | solution.py:75
  235.3 3.9 %copy.73 = bf16[2,16,64,768]{3,2,1,0:T(8,128)(2,1)} copy(bf16[2,16,64,768]{3,2,0,1:T(8,128)(2,1)} %bitcast.70) | data formatting | bytes 6291456 | tf_op jit(solution)/shard_map/transpose | solution.py:24
  239.3 10.2 %reduce-scatter.3.cloned.1.call-done = bf16[16,64,768]{2,1,0:T(8,128)(2,1)} async-done(((bf16[32,64,768]{2,1,0:T(8,128)(2,1)}), bf16[16,64,768]{2,1,0:T(8,128)(2,1)}) %reduce-scatter.3.cloned.1.call-update) | async-done | bytes 1572880 | tf_op jit(solution)/shard_map/reduce_scatter | solution.py:27
  249.5 66.0 %reduce-scatter.5.cloned.1.call-done = bf16[1,64,768]{2,1,0:T(8,128)(2,1)} async-done(((bf16[16,64,768]{2,1,0:T(8,128)(2,1)}), bf16[1,64,768]{2,1,0:T(8,128)(2,1)}) %reduce-scatter.5.cloned.1.call-update) | async-done | bytes 98320 | tf_op jit(solution)/shard_map/reduce_scatter | solution.py:27
  315.6 1.1 copy.79
  316.6 0.8 reshape.92
  317.4 6.6 %all-to-all-start.3 = ((bf16[16,2,1536]{2,1,0:T(2,128)(2,1)}), bf16[16,2,1536]{2,1,0:T(2,128)(2,1)S(1)}, u32[]{:S(2)}, u32[]{:S(2)}) async-start(bf16[16,2,1536]{2,1,0:T(2,128)(2,1)} %reshape.92), calls=%async_computation.5 | async-start | bytes 196608 | tf_op jit(solution)/shard_map/all_to_all | solution.py:83
  324.0 6.6 %all-to-all-done.3 = bf16[16,2,1536]{2,1,0:T(2,128)(2,1)S(1)} async-done(((bf16[16,2,1536]{2,1,0:T(2,128)(2,1)}), bf16[16,2,1536]{2,1,0:T(2,128)(2,1)S(1)}, u32[]{:S(2)}, u32[]{:S(2)}) %all-to-all-start.3) | async-done | bytes 98336 | tf_op jit(solution)/shard_map/all_to_all | solution.py:83
  330.7 0.2 reshape.93
  330.8 0.3 convolution_multiply_fusion.1
  331.1 0.3 multiply_reduce_fusion
  331.5 33.0 %all_to_all.40 = f32[32,1,256]{2,1,0:T(1,128)S(1)} all-to-all(f32[32,1,256]{2,1,0:T(1,128)S(1)} %broadcast_in_dim.5), channel_id=1, replica_groups=mesh['ep'=16,'tp_0'=16,'tp_1'=2] {'tp_0','tp_1'}, dimensions={0} | all-to-all | bytes 65536 | tf_op jit(solution)/shard_map/all_to_all | solution.py:13
  364.6 0.7 multiply_convert_fusion
  (33 shorter events, 1.3 us)
Async XLA Ops:
  6.5 221.4 %copy-start = (bf16[1,256,2048]{2,1,0:T(8,128)(2,1)S(1)}, bf16[1,256,2048]{2,1,0:T(8,128)(2,1)}, u32[]{:S(2)}) copy-start(bf16[1,256,2048]{2,1,0:T(8,128)(2,1)} %param.12) | copy-start | bytes 3145732
  8.0 28.8 %all-to-all-start = ((f32[32,1,256]{2,1,0:T(1,128)}), f32[32,1,256]{2,1,0:T(1,128)S(1)}, u32[]{:S(2)}, u32[]{:S(2)}) async-start(f32[32,1,256]{2,1,0:T(1,128)} %broadcast_in_dim.4), calls=%async_computation | async-start | bytes 65536 | tf_op jit(solution)/shard_map/all_to_all | solution.py:13
  24.8 224.7 %reduce-scatter.3.cloned.1.call-start = ((), (), s32[]{:S(2)}) async-start(), calls=%async_computation.7 | async-start | bytes 4718592 | tf_op jit(solution)/shard_map/reduce_scatter | solution.py:27
  214.0 9.8 %copy-start.4 = (bf16[1,2048,256]{2,1,0:T(8,128)(2,1)S(1)}, bf16[1,2048,256]{2,1,0:T(8,128)(2,1)}, u32[]{:S(2)}) copy-start(bf16[1,2048,256]{2,1,0:T(8,128)(2,1)} %param.10) | copy-start | bytes 3145732
  223.8 3.1 copy-start.1
  223.8 3.1 copy-start.5
  239.2 84.8 %copy-start.2 = (f32[256,2]{0,1:T(2,128)S(1)}, f32[256,2]{0,1:T(2,128)}, u32[]{:S(2)}) copy-start(f32[256,2]{0,1:T(2,128)} %param.14) | copy-start | bytes 6148
  239.2 125.3 %copy-start.3 = (f32[64]{0:T(128)S(1)}, f32[64]{0:T(128)}, u32[]{:S(2)}) copy-start(f32[64]{0:T(128)} %param.15) | copy-start | bytes 772
  239.3 76.3 %reduce-scatter.5.cloned.1.call-start = ((), (), s32[]{:S(2)}) async-start(), calls=%async_computation.8 | async-start | bytes 1671168 | tf_op jit(solution)/shard_map/reduce_scatter | solution.py:27
  317.4 13.2 %all-to-all-start.3 = ((bf16[16,2,1536]{2,1,0:T(2,128)(2,1)}), bf16[16,2,1536]{2,1,0:T(2,128)(2,1)S(1)}, u32[]{:S(2)}, u32[]{:S(2)}) async-start(bf16[16,2,1536]{2,1,0:T(2,128)(2,1)} %reshape.92), calls=%async_computation.5 | async-start | bytes 196608 | tf_op jit(solution)/shard_map/all_to_all | solution.py:83
Sparse Core Ops, SparseCore 0:
  239.4 10.0 reduce-scatter.2
  252.3 63.1 reduce-scatter.4
